TPU v7x, 32 devices: a whole 2x2x4 slice. The times are simulated.
32 devices in a mesh: ep: 4 (over y, x), tp: 8 (over z, core).
Axes of the slice: x: 2, y: 2, z: 4, core: 2. Of those that a mesh axis runs over, the one named last changes fastest.
Arguments:
- residual: bfloat16 [128, 2048], P('ep'), may hold values from -20 to 20
- cache_latent: bfloat16 [128, 2048, 256], P(('ep', 'tp')), may hold values from -12 to 12
- cache_rope: bfloat16 [128, 32, 2048], P(('ep', 'tp')), may hold values from -6 to 6
- lengths: int32 [128], P(('ep', 'tp')), may hold values from 2 to 2048, as said below
- query_latent: bfloat16 [128, 32, 256], P(('ep', 'tp')), may hold values from -250 to 250
- query_rope: bfloat16 [128, 32, 32], P(('ep', 'tp')), may hold values from -6 to 6
- norm_gain: bfloat16 [2048], replicated, may hold values from 0.099609375 to 1.8984375
- latent_weight: bfloat16 [2048, 256], replicated, may hold values from -0.125 to 0.125
- latent_gain: bfloat16 [256], replicated, may hold values from 0.099609375 to 1.8984375
- rope_weight: bfloat16 [32, 2048], replicated, may hold values from -0.125 to 0.125
- value_weight: bfloat16 [256, 2048], replicated, may hold values from -0.375 to 0.375
- out_weight: bfloat16 [2048, 2048], P('tp'), may hold values from -1 to 1
- mixer_gain: bfloat16 [2048], replicated, may hold values from 0.099609375 to 1.8984375
- group_router: bfloat16 [2048, 4], replicated, may hold values from -0.0625 to 0.0625
- expert_router: bfloat16 [2048, 8], replicated, may hold values from -0.0625 to 0.0625
- expert_ids: int32 [128, 2], P('ep'), may hold values from 0 to 7, as said below
- gate_weight: bfloat16 [8, 2048, 4096], P('ep', None, 'tp'), may hold values from -0.125 to 0.125
- up_weight: bfloat16 [8, 2048, 4096], P('ep', None, 'tp'), may hold values from -0.125 to 0.125
- down_weight: bfloat16 [8, 4096, 2048], P('ep', 'tp'), may hold values from -0.75 to 0.75
Outputs:
- mixed: bfloat16 [128, 2048], P('ep')
- new_latent: bfloat16 [128, 256], P(('ep', 'tp'))
- new_rope_key: bfloat16 [128, 32], P(('ep', 'tp'))
Inputs may be any that keep to these rules, and one draw needn't show every extreme that they name: `lengths`: every sequence has 2 or more cached positions, and in every draw some sequence has all 2048. `expert_ids`: each row names 2 different experts of one group; group g holds experts g * 2 to g * 2 + 1. Among the rows of one index of ep (aligned blocks of 32 rows) no expert is named more than 16 times, and in every draw some expert is named exactly 16 times in every block.
All inputs are finite; a program needn't handle non-finite values.
Results may differ from a plain program's by a relative error of at most 0.012.
Values may be sent and summed in bfloat16 or wider, within the bound.
A program may use at most 64 MiB of HBM per device.

v0:
```python
import jax
import jax.numpy as jnp
from jax import lax
from jax.sharding import PartitionSpec as P

H = 32
KV = 256
ROPE = 32
NOPE = 64
V = 64
GROUPS = 4
TOPK = 2
NORM_EPSILON = 1e-06
ROPE_BASE = 10000.0


def inverse_rms(values):
    return lax.rsqrt(jnp.mean(values * values, axis=-1, keepdims=True) + NORM_EPSILON)


def rotate(vector, position):
    half_width = vector.shape[-1] // 2
    frequency = ROPE_BASE ** (
        -jnp.arange(0, vector.shape[-1], 2, dtype=jnp.float32) / vector.shape[-1]
    )
    angles = position[..., None] * frequency
    lower_half = vector[..., :half_width]
    upper_half = vector[..., half_width:]
    return jnp.concatenate(
        [
            lower_half * jnp.cos(angles) - upper_half * jnp.sin(angles),
            upper_half * jnp.cos(angles) + lower_half * jnp.sin(angles),
        ],
        axis=-1,
    )


def dispatch_table(expert_rows, experts, capacity):
    flat_ids = expert_rows.reshape(-1)
    hit_table = (flat_ids[:, None] == jnp.arange(experts, dtype=jnp.int32)[None, :]).astype(
        jnp.int32
    )
    slot_rank = jnp.sum((jnp.cumsum(hit_table, axis=0) - hit_table) * hit_table, axis=1)
    slot_index = flat_ids * capacity + slot_rank
    picked = (
        slot_index[None, :] == jnp.arange(experts * capacity, dtype=jnp.int32)[:, None]
    ).astype(jnp.float32)
    return picked.reshape(experts * capacity, expert_rows.shape[0], expert_rows.shape[1])


def route_weights(expert_in, group_router, expert_router, expert_ids, per_group):
    group_logits = jnp.dot(expert_in, group_router, preferred_element_type=jnp.float32)
    expert_logits = jnp.dot(expert_in, expert_router, preferred_element_type=jnp.float32)
    chosen = expert_ids[:, 0] // per_group
    group_hit = (
        jnp.arange(group_logits.shape[1], dtype=jnp.int32)[None, :] == chosen[:, None]
    ).astype(jnp.float32)
    chosen_logit = jnp.sum(group_logits * group_hit, axis=1, keepdims=True)
    group_share = 1.0 / jnp.sum(jnp.exp(group_logits - chosen_logit), axis=1)
    expert_hit = (
        expert_ids[:, :, None] == jnp.arange(expert_logits.shape[1], dtype=jnp.int32)[None, None, :]
    ).astype(jnp.float32)
    picked_logit = jnp.sum(expert_hit * expert_logits[:, None, :], axis=2)
    inner_share = 1.0 / jnp.sum(
        jnp.exp(picked_logit[:, None, :] - picked_logit[:, :, None]), axis=2
    )
    return group_share[:, None] * inner_share


def on_device(
    residual,
    cache_latent,
    cache_rope,
    lengths,
    query_latent,
    query_rope,
    norm_gain,
    latent_weight,
    latent_gain,
    rope_weight,
    value_weight,
    out_weight,
    mixer_gain,
    group_router,
    expert_router,
    expert_ids,
    gate_weight,
    up_weight,
    down_weight,
):
    ep_count = lax.axis_size("ep")
    seq_count = cache_latent.shape[0]
    group_rows = residual.shape[0]
    model_width = residual.shape[1]
    resid_f = residual.astype(jnp.float32)
    own_rows = lax.dynamic_slice_in_dim(resid_f, lax.axis_index("tp") * seq_count, seq_count, 0)
    normed = (own_rows * inverse_rms(own_rows) * norm_gain.astype(jnp.float32)).astype(jnp.bfloat16)
    latent_raw = jnp.dot(normed, latent_weight, preferred_element_type=jnp.float32)
    new_latent = (latent_raw * inverse_rms(latent_raw) * latent_gain.astype(jnp.float32)).astype(
        jnp.bfloat16
    )
    positions = lengths.astype(jnp.float32)
    rope_raw = jnp.dot(normed, rope_weight.T, preferred_element_type=jnp.float32)
    new_rope_key = rotate(rope_raw, positions).astype(jnp.bfloat16)
    query_turned = rotate(query_rope.astype(jnp.float32), positions[:, None]).astype(jnp.bfloat16)
    score_scale = (NOPE + ROPE) ** (-0.5)
    cached = (
        jnp.einsum("shc,spc->shp", query_latent, cache_latent, preferred_element_type=jnp.float32)
        + jnp.einsum("shr,srp->shp", query_turned, cache_rope, preferred_element_type=jnp.float32)
    ) * score_scale
    keeping = (
        jnp.arange(cache_latent.shape[1], dtype=jnp.int32)[None, None, :] < lengths[:, None, None]
    )
    cached = jnp.where(keeping, cached, -jnp.inf)
    fresh = (
        jnp.einsum("shc,sc->sh", query_latent, new_latent, preferred_element_type=jnp.float32)
        + jnp.einsum("shr,sr->sh", query_turned, new_rope_key, preferred_element_type=jnp.float32)
    ) * score_scale
    row_top = jnp.maximum(jnp.max(cached, axis=2), fresh)
    cached_exp = jnp.exp(cached - row_top[:, :, None])
    fresh_exp = jnp.exp(fresh - row_top)
    denominator = jnp.sum(cached_exp, axis=2) + fresh_exp
    cached_weight = (cached_exp / denominator[:, :, None]).astype(jnp.bfloat16)
    fresh_weight = (fresh_exp / denominator).astype(jnp.bfloat16)
    mixed_latent = (
        jnp.einsum("shp,spc->shc", cached_weight, cache_latent, preferred_element_type=jnp.float32)
        + fresh_weight.astype(jnp.float32)[:, :, None] * new_latent.astype(jnp.float32)[:, None, :]
    ).astype(jnp.bfloat16)
    head_values = jnp.einsum(
        "shc,chv->shv",
        mixed_latent,
        value_weight.reshape(KV, H, V),
        preferred_element_type=jnp.float32,
    ).astype(jnp.bfloat16)
    by_heads = lax.all_to_all(head_values, "tp", split_axis=1, concat_axis=0, tiled=True)
    head_terms = jnp.dot(
        by_heads.reshape(group_rows, -1), out_weight, preferred_element_type=jnp.float32
    )
    attended = lax.psum(head_terms, "tp")
    after_attention = (resid_f + attended).astype(jnp.bfloat16)
    after_f = after_attention.astype(jnp.float32)
    expert_in = (after_f * inverse_rms(after_f) * mixer_gain.astype(jnp.float32)).astype(
        jnp.bfloat16
    )
    experts = expert_router.shape[1]
    capacity = 2 * group_rows * TOPK // experts
    route_weight = route_weights(
        expert_in, group_router, expert_router, expert_ids, experts // GROUPS
    )
    picked = dispatch_table(expert_ids, experts, capacity)
    select_rows = jnp.sum(picked, axis=2).astype(jnp.bfloat16)
    outbound = jnp.dot(select_rows, expert_in, preferred_element_type=jnp.float32).astype(
        jnp.bfloat16
    )
    outbound = outbound.reshape(ep_count, gate_weight.shape[0], capacity, model_width)
    rows = lax.all_to_all(outbound, "ep", split_axis=0, concat_axis=0, tiled=True)
    gate_value = jnp.einsum("secd,edf->secf", rows, gate_weight, preferred_element_type=jnp.float32)
    up_value = jnp.einsum("secd,edf->secf", rows, up_weight, preferred_element_type=jnp.float32)
    activation = (jax.nn.silu(gate_value) * up_value).astype(jnp.bfloat16)
    expert_terms = jnp.einsum(
        "secf,efd->secd", activation, down_weight, preferred_element_type=jnp.float32
    )
    combine = jnp.sum(picked * route_weight[None, :, :], axis=2).T
    summed_terms = lax.psum_scatter(expert_terms, "tp", scatter_dimension=3, tiled=True)
    returned_terms = lax.all_to_all(summed_terms, "ep", split_axis=0, concat_axis=0, tiled=True)
    share_width = returned_terms.shape[3]
    moe_part = jnp.dot(
        combine, returned_terms.reshape(-1, share_width), precision=lax.Precision.HIGHEST
    )
    after_cols = lax.dynamic_slice_in_dim(
        after_f, lax.axis_index("tp") * share_width, share_width, 1
    )
    mixed_share = (after_cols + moe_part).astype(jnp.bfloat16)
    mixed = lax.all_gather(mixed_share, "tp", axis=1, tiled=True)
    return (mixed, new_latent, new_rope_key)


def solution(mesh):
    in_specs = (
        P("ep", None),
        P(("ep", "tp"), None, None),
        P(("ep", "tp"), None, None),
        P(("ep", "tp")),
        P(("ep", "tp"), None, None),
        P(("ep", "tp"), None, None),
        P(),
        P(),
        P(),
        P(),
        P(),
        P("tp", None),
        P(),
        P(),
        P(),
        P("ep", None),
        P("ep", None, "tp"),
        P("ep", None, "tp"),
        P("ep", "tp", None),
    )
    out_specs = (P("ep", None), P(("ep", "tp"), None), P(("ep", "tp"), None))
    return jax.shard_map(
        on_device, mesh=mesh, in_specs=in_specs, out_specs=out_specs, check_vma=False
    )
```

profile of v0, /device:TPU:0, one launch (start us, length us, event | category | flops | bytes accessed | tf_op | source)
XLA Modules:
  0.0 177.1 jit_solution(6395437696958432695)
XLA Ops:
  7.2 0.0 copy-start
  7.2 0.0 copy-start.3
  7.2 0.8 convert_element_type.79
  8.0 0.7 iota_compare_fusion.2
  8.7 0.9 convert_element_type.77
  9.7 0.1 multiply_reduce_fusion.1
  9.8 0.7 convert_element_type.80
  10.5 0.8 convert_element_type.78
  11.3 1.1 fusion.50
  12.4 1.6 multiply_reduce_fusion.2
  14.0 0.7 convert_element_type.82
  14.7 3.5 %fusion.58 = f32[4,32,2048]{2,1,0:T(8,128)S(1)} fusion(bf16[4,32,256]{2,1,0:T(8,128)(2,1)} %param.23, bf16[4,2048,256]{2,1,0:T(8,128)(2,1)} %param.20), kind=kOutput, calls=%fused_computation.90 | convolution fusion | flops 134217728 | bytes 5308416 | tf_op jit(solution)/shard_map/shc,spc->shp/dot_general | solution.py:108
  18.2 0.1 fusion.53
  18.3 0.1 fusion.40
  18.4 0.1 subtract_convert_fusion.1
  18.6 0.1 fusion.79
  18.6 0.1 subtract_convert_fusion
  18.7 0.2 fusion.39
  18.9 0.5 fusion.54
  19.4 0.3 fusion.26
  19.8 1.5 copy.61
  21.2 0.0 copy-start.5
  21.3 0.0 copy-start.6
  21.3 0.0 copy-start.1
  21.3 0.0 copy-start.8
  21.3 0.0 copy-start.4
  21.3 3.1 %fusion.23 = bf16[4,32,256]{2,1,0:T(8,128)(2,1)S(1)} fusion(bf16[4,2048,256]{2,1,0:T(8,128)(2,1)} %param.20, f32[4,32,2048]{2,1,0:T(8,128)S(1)} %get-tuple-element.18, f32[4,32]{1,0:T(4,128)S(1)} %get-tuple-element.12, f32[4,32]{1,0:T(4,128)S(1)} %fusion.44, f32[4,256]{1,0:T(4,128)S(1)} %get-tuple-element.7, f32[4,32]{1,0:T(4,128)S(1)} %get-tuple-element.11), kind=kOutput, calls=%fused_computation.16 | convolution fusion | flops 135102464 | bytes 5314048 | tf_op jit(solution)/shard_map/shp,spc->shc/dot_general | solution.py:126
  24.4 0.0 copy-done.7
  24.4 0.4 fusion.55
  24.8 0.7 reshape.194
  25.5 6.4 %all-to-all-start = ((bf16[8,2,512]{2,1,0:T(2,128)(2,1)}), bf16[8,2,512]{2,1,0:T(2,128)(2,1)S(1)}, u32[]{:S(2)}, u32[]{:S(2)}) async-start(bf16[8,2,512]{2,1,0:T(2,128)(2,1)} %reshape.194), calls=%async_computation | async-start | bytes 32768 | tf_op jit(solution)/shard_map/all_to_all | solution.py:135
  31.9 0.0 all-reduce.2.cloned.1.call-start
  31.9 0.1 copy.64
  32.0 0.1 eq.57
  32.1 0.1 fusion.37
  32.2 0.1 reduce_window_sum.11
  32.3 0.2 select_reduce_fusion.1
  32.5 0.1 reduce_sum.105
  32.6 0.1 copy.65
  32.7 4.8 %all-to-all-done = bf16[8,2,512]{2,1,0:T(2,128)(2,1)S(1)} async-done(((bf16[8,2,512]{2,1,0:T(2,128)(2,1)}), bf16[8,2,512]{2,1,0:T(2,128)(2,1)S(1)}, u32[]{:S(2)}, u32[]{:S(2)}) %all-to-all-start) | async-done | bytes 16416 | tf_op jit(solution)/shard_map/all_to_all | solution.py:135
  37.5 0.1 reshape.195
  37.6 0.1 reshape.184
  37.7 1.0 fusion.59
  38.7 0.0 all-reduce.2.cloned.1.call-update
  38.7 0.0 reduce-scatter.2.cloned.1.call-start
  38.8 53.8 %all-reduce.2.cloned.1.call-done = f32[32,2048]{1,0:T(8,128)} async-done(((f32[32,2048]{1,0:T(8,128)}), f32[32,2048]{1,0:T(8,128)}) %all-reduce.2.cloned.1.call-update) | async-done | bytes 262160 | tf_op jit(solution)/shard_map/psum | solution.py:139
  92.6 1.1 multiply_reduce_fusion
  93.7 0.1 multiply_convert_fusion
  93.8 0.2 select_reduce_fusion.3
  94.0 0.1 fusion.60
  94.2 0.1 convert_reduce_fusion
  94.3 0.3 convolution_convert_fusion
  94.6 10.6 %all_to_all.25 = bf16[4,2,16,2048]{3,2,1,0:T(8,128)(2,1)S(1)} all-to-all(bf16[4,2,16,2048]{3,2,1,0:T(8,128)(2,1)S(1)} %bitcast.81), channel_id=1, replica_groups=mesh['ep'=4,'tp'=8] {'ep'}, dimensions={0} | all-to-all | bytes 1048576 | tf_op jit(solution)/shard_map/all_to_all | solution.py:156
  105.2 3.0 %fusion.11 = f32[4,2,16,512]{3,2,0,1:T(8,128)S(1)} fusion(bf16[2,2048,512]{2,1,0:T(8,128)(2,1)} %param.35, bf16[4,2,16,2048]{3,2,1,0:T(8,128)(2,1)S(1)} %all_to_all.25), kind=kOutput, calls=%fused_computation.11 | convolution fusion | flops 268435456 | bytes 4980736 | tf_op jit(solution)/shard_map/secd,edf->secf/dot_general | solution.py:157
  108.2 6.0 %fusion.6 = f32[4,2,16,2048]{3,2,0,1:T(8,128)} fusion(bf16[2,512,2048]{2,1,0:T(8,128)(2,1)} %param.37, bf16[2,2048,512]{2,1,0:T(8,128)(2,1)} %param.36, bf16[4,2,16,2048]{3,2,1,0:T(8,128)(2,1)S(1)} %all_to_all.25, f32[4,2,16,512]{3,2,0,1:T(8,128)S(1)} %fusion.11), kind=kOutput, calls=%fused_computation.6 | convolution fusion | flops 537264128 | bytes 10223616 | tf_op jit(solution)/shard_map/secf,efd->secd/dot_general | solution.py:160
  114.3 0.0 reduce-scatter.2.cloned.1.call-update
  114.3 30.9 %reduce-scatter.2.cloned.1.call-done = f32[4,2,16,256]{3,2,0,1:T(8,128)} async-done(((f32[4,2,16,2048]{3,2,0,1:T(8,128)}), f32[4,2,16,256]{3,2,0,1:T(8,128)}) %reduce-scatter.2.cloned.1.call-update) | async-done | bytes 131088 | tf_op jit(solution)/shard_map/reduce_scatter | solution.py:164
  145.2 1.6 copy.68
  146.8 3.7 %all-to-all-start.2 = ((f32[4,2,16,256]{3,2,1,0:T(8,128)}), f32[4,2,16,256]{3,2,1,0:T(8,128)S(1)}, u32[]{:S(2)}, u32[]{:S(2)}) async-start(f32[4,2,16,256]{3,2,1,0:T(8,128)} %copy.68), calls=%async_computation.3 | async-start | bytes 262144 | tf_op jit(solution)/shard_map/all_to_all | solution.py:165
  150.4 0.6 pad_maximum_fusion.3
  151.1 4.4 %all-to-all-done.2 = f32[4,2,16,256]{3,2,1,0:T(8,128)S(1)} async-done(((f32[4,2,16,256]{3,2,1,0:T(8,128)}), f32[4,2,16,256]{3,2,1,0:T(8,128)S(1)}, u32[]{:S(2)}, u32[]{:S(2)}) %all-to-all-start.2) | async-done | bytes 131104 | tf_op jit(solution)/shard_map/all_to_all | solution.py:165
  155.5 0.2 fusion.25
  155.6 14.0 %all_gather.3 = bf16[32,2048]{1,0:T(8,128)(2,1)S(1)} all-gather(bf16[32,256]{1,0:T(8,128)(2,1)S(1)} %fusion.25), channel_id=1, replica_groups=mesh['ep'=4,'tp'=8] {'tp'}, dimensions={1}, use_global_device_ids=true | all-gather | bytes 147456 | tf_op jit(solution)/shard_map/all_gather | solution.py:174
  169.6 0.7 copy.94
  (25 shorter events, 0.2 us)
Async XLA Ops:
  7.2 30.6 %copy-start = (bf16[256,2048]{1,0:T(8,128)(2,1)S(1)}, bf16[256,2048]{1,0:T(8,128)(2,1)}, u32[]{:S(2)}) copy-start(bf16[256,2048]{1,0:T(8,128)(2,1)} %param.30) | copy-start | bytes 3145732
  7.2 11.1 %copy-start.3 = (bf16[4,32,256]{2,1,0:T(8,128)(2,1)S(1)}, bf16[4,32,256]{2,1,0:T(8,128)(2,1)}, u32[]{:S(2)}) copy-start(bf16[4,32,256]{2,1,0:T(8,128)(2,1)} %param.23) | copy-start | bytes 196612
  7.2 11.7 %copy-start.2 = (bf16[4,32,2048]{2,1,0:T(8,128)(2,1)S(1)}, bf16[4,32,2048]{2,1,0:T(8,128)(2,1)}, u32[]{:S(2)}) copy-start(bf16[4,32,2048]{2,1,0:T(8,128)(2,1)} %param.21) | copy-start | bytes 1572868
  18.3 6.1 %copy-start.7 = (bf16[4,256]{1,0:T(4,128)(2,1)}, bf16[4,256]{1,0:T(4,128)(2,1)S(1)}, u32[]{:S(2)}) copy-start(bf16[4,256]{1,0:T(4,128)(2,1)S(1)} %get-tuple-element.27) | copy-start | bytes 6148
  21.2 10.7 %copy-start.5 = (s32[32,2]{0,1:T(2,128)S(1)}, s32[32,2]{0,1:T(2,128)}, u32[]{:S(2)}) copy-start(s32[32,2]{0,1:T(2,128)} %param.34) | copy-start | bytes 772
  21.3 11.4 %copy-start.6 = (bf16[2048]{0:T(1024)(128)(2,1)S(1)}, bf16[2048]{0:T(1024)(128)(2,1)}, u32[]{:S(2)}) copy-start(bf16[2048]{0:T(1024)(128)(2,1)} %param.31) | copy-start | bytes 12292
  21.3 71.3 %copy-start.1 = (bf16[32,2048]{1,0:T(8,128)(2,1)S(1)}, bf16[32,2048]{1,0:T(8,128)(2,1)}, u32[]{:S(2)}) copy-start(bf16[32,2048]{1,0:T(8,128)(2,1)} %param.19) | copy-start | bytes 393220
  21.3 72.5 %copy-start.8 = (bf16[2048,4]{0,1:T(4,128)(2,1)S(1)}, bf16[2048,4]{0,1:T(4,128)(2,1)}, u32[]{:S(2)}) copy-start(bf16[2048,4]{0,1:T(4,128)(2,1)} %param.32) | copy-start | bytes 49156
  21.3 72.7 %copy-start.4 = (bf16[2048,8]{0,1:T(8,128)(2,1)S(1)}, bf16[2048,8]{0,1:T(8,128)(2,1)}, u32[]{:S(2)}) copy-start(bf16[2048,8]{0,1:T(8,128)(2,1)} %param.33) | copy-start | bytes 98308
  25.5 12.0 %all-to-all-start = ((bf16[8,2,512]{2,1,0:T(2,128)(2,1)}), bf16[8,2,512]{2,1,0:T(2,128)(2,1)S(1)}, u32[]{:S(2)}, u32[]{:S(2)}) async-start(bf16[8,2,512]{2,1,0:T(2,128)(2,1)} %reshape.194), calls=%async_computation | async-start | bytes 32768 | tf_op jit(solution)/shard_map/all_to_all | solution.py:135
  31.9 60.7 %all-reduce.2.cloned.1.call-start = ((), (), s32[]{:S(2)}) async-start(), calls=%async_computation.4 | async-start | bytes 524288 | tf_op jit(solution)/shard_map/psum | solution.py:139
  38.7 106.5 %reduce-scatter.2.cloned.1.call-start = ((), (), s32[]{:S(2)}) async-start(), calls=%async_computation.5 | async-start | bytes 1179648 | tf_op jit(solution)/shard_map/reduce_scatter | solution.py:164
  146.8 8.7 %all-to-all-start.2 = ((f32[4,2,16,256]{3,2,1,0:T(8,128)}), f32[4,2,16,256]{3,2,1,0:T(8,128)S(1)}, u32[]{:S(2)}, u32[]{:S(2)}) async-start(f32[4,2,16,256]{3,2,1,0:T(8,128)} %copy.68), calls=%async_computation.3 | async-start | bytes 262144 | tf_op jit(solution)/shard_map/all_to_all | solution.py:165
Sparse Core Ops, SparseCore 0:
  38.9 53.6 all-reduce.1
  114.4 30.7 reduce-scatter.1
where the time goes:
time: 178 us; the launch traced here: 177 us
  waiting for transfers between devices  93.9 us (53%)
  blocking collectives  24.5 us (14%)
  matrix products  21.4 us (12%)
  between operations  14.3 us (8%)
  starting transfers between devices  10.1 us (6%)
  other arithmetic  7.81 us (4%)
  local copies, waits for them, and re-layouts  5.06 us (3%)
    psum x1, waiting for transfers between devices, on_device(): attended = lax.psum(head_terms, 'tp')  53.8 us
    reduce_scatter x1, waiting for transfers between devices, on_device(): lax.psum_scatter(expert_terms, 'tp', scatter_dimension=3, tiled=True)  30.9 us
    all_gather x1, blocking collectives, on_device(): mixed = lax.all_gather(mixed_share, 'tp', axis=1, tiled=True)  14 us
    all_to_all x1, blocking collectives, on_device(): lax.all_to_all(outbound, 'ep', split_axis=0, concat_axis=0, tiled=True)  10.6 us
    all_to_all x1, starting transfers between devices, on_device(): lax.all_to_all(head_values, 'tp', split_axis=1, concat_axis=0, tiled=True)  6.35 us
    dot_general x1, matrix products, on_device(): jnp.einsum('secf,efd->secd', activation, down_weight, preferred_element_t...  6.04 us
    all_to_all x1, waiting for transfers between devices, on_device(): lax.all_to_all(head_values, 'tp', split_axis=1, concat_axis=0, tiled=True)  4.83 us
    all_to_all x1, waiting for transfers between devices, on_device(): lax.all_to_all(summed_terms, 'ep', split_axis=0, concat_axis=0, tiled=True)  4.38 us
  transfers between devices with their start and end apart: 4, of which 4 were waited for; matrix products, arithmetic and copies ran while one was open for 1% of the time, Pallas kernels for 0%

commit v1 on v0

--- a/solution.py
+++ b/solution.py
@@ -12,6 +12,15 @@
 TOPK = 2
 NORM_EPSILON = 1e-06
 ROPE_BASE = 10000.0
+
+
+def add_in_pairs(x, axis):
+    size = lax.axis_size(axis)
+    total, stride = (x, 1)
+    while stride < size:
+        total = total + lax.ppermute(total, axis, [(i, i ^ stride) for i in range(size)])
+        stride = 2 * stride
+    return total
 
 
 def inverse_rms(values):
@@ -136,7 +145,7 @@
     head_terms = jnp.dot(
         by_heads.reshape(group_rows, -1), out_weight, preferred_element_type=jnp.float32
     )
-    attended = lax.psum(head_terms, "tp")
+    attended = add_in_pairs(head_terms, "tp")
     after_attention = (resid_f + attended).astype(jnp.bfloat16)
     after_f = after_attention.astype(jnp.float32)
     expert_in = (after_f * inverse_rms(after_f) * mixer_gain.astype(jnp.float32)).astype(

time: 178 us -> 146 us (0.82)
  waiting for transfers between devices: 93.9 us -> 55.8 us
  blocking collectives: 24.5 us -> 37.9 us
  starting transfers between devices: 10.1 us -> 5.08 us
    psum x1 -> x0, waiting for transfers between devices: 53.8 us -> none  [on_device(): attended = lax.psum(head_terms, 'tp')]
    ppermute x0 -> x3, waiting for transfers between devices: none -> 22 us  [add_in_pairs(): lax.ppermute(total, axis, [(i, i ^ stride) for i in range(size)])]
    all_to_all x0 -> x1, blocking collectives: none -> 11.8 us  [on_device(): lax.all_to_all(head_values, 'tp', split_axis=1, concat_axis=0, tiled=True)]
    all_to_all x1 -> x0, starting transfers between devices: 6.35 us -> none  [on_device(): lax.all_to_all(head_values, 'tp', split_axis=1, concat_axis=0, tiled=True)]
    all_to_all x1 -> x0, waiting for transfers between devices: 4.83 us -> none  [on_device(): lax.all_to_all(head_values, 'tp', split_axis=1, concat_axis=0, tiled=True)]
  transfers between devices with their start and end apart: 4 -> 5, of which waited for: 4 -> 5; matrix products, arithmetic and copies ran while one was open for 1% -> 1% of each run, Pallas kernels for 0% -> 0%
where the time goes in v1:
time: 146 us; the launch traced here: 145 us
  waiting for transfers between devices  55.8 us (38%)
  blocking collectives  37.9 us (26%)
  matrix products  20.6 us (14%)
  between operations  14.3 us (10%)
  other arithmetic  6.9 us (5%)
  starting transfers between devices  5.08 us (3%)
  local copies, waits for them, and re-layouts  4.44 us (3%)
    reduce_scatter x1, waiting for transfers between devices, on_device(): lax.psum_scatter(expert_terms, 'tp', scatter_dimension=3, tiled=True)  29.4 us
    ppermute x3, waiting for transfers between devices, add_in_pairs(): lax.ppermute(total, axis, [(i, i ^ stride) for i in range(size)])  22 us
    all_gather x1, blocking collectives, on_device(): mixed = lax.all_gather(mixed_share, 'tp', axis=1, tiled=True)  14 us
    all_to_all x1, blocking collectives, on_device(): lax.all_to_all(outbound, 'ep', split_axis=0, concat_axis=0, tiled=True)  12.2 us
    all_to_all x1, blocking collectives, on_device(): lax.all_to_all(head_values, 'tp', split_axis=1, concat_axis=0, tiled=True)  11.8 us
    dot_general x1, matrix products, on_device(): jnp.einsum('secf,efd->secd', activation, down_weight, preferred_element_t...  6.04 us
    all_to_all x1, waiting for transfers between devices, on_device(): lax.all_to_all(summed_terms, 'ep', split_axis=0, concat_axis=0, tiled=True)  4.38 us
    all_to_all x1, starting transfers between devices, on_device(): lax.all_to_all(summed_terms, 'ep', split_axis=0, concat_axis=0, tiled=True)  3.72 us
  transfers between devices with their start and end apart: 5, of which 5 were waited for; matrix products, arithmetic and copies ran while one was open for 1% of the time, Pallas kernels for 0%

profile of v1, /device:TPU:0, one launch (start us, length us, event | category | flops | bytes accessed | tf_op | source)
XLA Modules:
  0.0 145.1 jit_solution(1161917468706852740)
XLA Ops:
  7.2 0.0 copy-start
  7.2 0.0 copy-start.3
  7.2 0.0 reduce-scatter.2.cloned.1.call-start
  7.3 0.8 convert_element_type.79
  8.0 0.7 iota_compare_fusion.2
  8.8 0.9 convert_element_type.77
  9.7 0.1 multiply_reduce_fusion.1
  9.9 0.7 convert_element_type.80
  10.5 0.8 convert_element_type.78
  11.3 1.1 fusion.49
  12.4 1.6 %multiply_reduce_fusion.2 = (f32[4]{0:T(128)S(1)}, f32[4,256]{1,0:T(4,128)S(1)}) fusion(bf16[2048,256]{1,0:T(8,128)(2,1)} %param.26, f32[32,2048]{1,0:T(8,128)S(1)} %convert_element_type.77, s32[]{:T(128)S(6)} %select_n.17, f32[2048]{0:T(1024)S(1)} %convert_element_type.80, f32[4]{0:T(128)S(1)} %add_rsqrt_fusion.2), kind=kOutput, calls=%fused_computation.52 | convolution fusion | flops 4220924 | bytes 1094164 | tf_op jit(solution)/shard_map/dot_general | solution.py:107
  14.1 0.7 convert_element_type.82
  14.7 3.5 %fusion.57 = f32[4,32,2048]{2,1,0:T(8,128)S(1)} fusion(bf16[4,32,256]{2,1,0:T(8,128)(2,1)} %param.23, bf16[4,2048,256]{2,1,0:T(8,128)(2,1)} %param.20), kind=kOutput, calls=%fused_computation.89 | convolution fusion | flops 134217728 | bytes 5308416 | tf_op jit(solution)/shard_map/shc,spc->shp/dot_general | solution.py:117
  18.3 0.1 fusion.52
  18.4 0.1 fusion.39
  18.5 0.1 subtract_convert_fusion.1
  18.6 0.1 fusion.78
  18.7 0.1 subtract_convert_fusion
  18.8 0.2 fusion.38
  19.0 0.5 fusion.53
  19.5 0.3 fusion.25
  19.8 1.5 %copy.61 = bf16[256,2048]{0,1:T(8,128)(2,1)S(1)} copy(bf16[256,2048]{1,0:T(8,128)(2,1)} %param.29) | data formatting | bytes 2097152 | tf_op args[10]
  21.3 0.0 copy-start.6
  21.3 0.0 copy-start.1
  21.3 3.0 %fusion.23 = bf16[4,32,256]{2,1,0:T(8,128)(2,1)S(1)} fusion(bf16[4,2048,256]{2,1,0:T(8,128)(2,1)} %param.20, f32[4,32,2048]{2,1,0:T(8,128)S(1)} %get-tuple-element.18, f32[4,32]{1,0:T(4,128)S(1)} %get-tuple-element.12, f32[4,32]{1,0:T(4,128)S(1)} %fusion.43, f32[4,256]{1,0:T(4,128)S(1)} %get-tuple-element.7, f32[4,32]{1,0:T(4,128)S(1)} %get-tuple-element.11), kind=kOutput, calls=%fused_computation.16 | convolution fusion | flops 135102464 | bytes 5314048 | tf_op jit(solution)/shard_map/shp,spc->shc/dot_general | solution.py:135
  24.4 0.0 copy-start.8
  24.4 0.0 copy-start.4
  24.4 0.4 fusion.54
  24.8 0.1 reshape.194
  24.9 11.8 %all_to_all.25 = bf16[8,2,512]{2,1,0:T(2,128)(2,1)S(1)} all-to-all(bf16[8,2,512]{2,1,0:T(2,128)(2,1)S(1)} %reshape.194), channel_id=1, replica_groups=mesh['ep'=4,'tp'=8] {'tp'}, dimensions={0} | all-to-all | bytes 32768 | tf_op jit(solution)/shard_map/all_to_all | solution.py:144
  36.7 0.1 reshape.195
  36.8 0.1 reshape.184
  36.9 0.3 fusion.58
  37.2 0.0 collective-permute-start
  37.3 0.1 copy.64
  37.4 0.1 eq.57
  37.5 1.3 collective-permute-done
  38.8 0.7 collective-permute-start.1
  39.5 0.1 fusion.36
  39.6 0.1 reduce_window_sum.11
  39.7 7.6 %collective-permute-done.1 = f32[32,2048]{1,0:T(8,128)S(1)} collective-permute-done((f32[32,2048]{1,0:T(8,128)S(1)}, f32[32,2048]{1,0:T(8,128)S(1)}, u32[]{:S(2)}, u32[]{:S(2)}) %collective-permute-start.1) | collective-permute-done | bytes 262176 | tf_op jit(solution)/shard_map/ppermute | solution.py:21
  47.3 0.6 collective-permute-start.2
  47.9 0.2 select_reduce_fusion.1
  48.1 0.1 reduce_sum.105
  48.2 0.1 copy.65
  48.3 13.1 %collective-permute-done.2 = f32[32,2048]{1,0:T(8,128)S(1)} collective-permute-done((f32[32,2048]{1,0:T(8,128)S(1)}, f32[32,2048]{1,0:T(8,128)S(1)}, u32[]{:S(2)}, u32[]{:S(2)}) %collective-permute-start.2) | collective-permute-done | bytes 262176 | tf_op jit(solution)/shard_map/ppermute | solution.py:21
  61.3 0.2 multiply_reduce_fusion
  61.5 0.1 multiply_convert_fusion
  61.6 0.2 select_reduce_fusion.3
  61.8 0.1 fusion.59
  62.1 0.1 convert_reduce_fusion
  62.2 0.3 convolution_convert_fusion
  62.5 12.2 %all_to_all.26 = bf16[4,2,16,2048]{3,2,1,0:T(8,128)(2,1)S(1)} all-to-all(bf16[4,2,16,2048]{3,2,1,0:T(8,128)(2,1)S(1)} %bitcast.81), channel_id=1, replica_groups=mesh['ep'=4,'tp'=8] {'ep'}, dimensions={0} | all-to-all | bytes 1048576 | tf_op jit(solution)/shard_map/all_to_all | solution.py:165
  74.6 3.0 %fusion.11 = f32[4,2,16,512]{3,2,0,1:T(8,128)S(1)} fusion(bf16[2,2048,512]{2,1,0:T(8,128)(2,1)} %param.35, bf16[4,2,16,2048]{3,2,1,0:T(8,128)(2,1)S(1)} %all_to_all.26), kind=kOutput, calls=%fused_computation.11 | convolution fusion | flops 268435456 | bytes 4980736 | tf_op jit(solution)/shard_map/secd,edf->secf/dot_general | solution.py:166
  77.7 6.0 %fusion.6 = f32[4,2,16,2048]{3,2,0,1:T(8,128)} fusion(bf16[2,512,2048]{2,1,0:T(8,128)(2,1)} %param.37, bf16[2,2048,512]{2,1,0:T(8,128)(2,1)} %param.36, bf16[4,2,16,2048]{3,2,1,0:T(8,128)(2,1)S(1)} %all_to_all.26, f32[4,2,16,512]{3,2,0,1:T(8,128)S(1)} %fusion.11), kind=kOutput, calls=%fused_computation.6 | convolution fusion | flops 537264128 | bytes 10223616 | tf_op jit(solution)/shard_map/secf,efd->secd/dot_general | solution.py:169
  83.7 0.0 reduce-scatter.2.cloned.1.call-update
  83.7 29.4 %reduce-scatter.2.cloned.1.call-done = f32[4,2,16,256]{3,2,0,1:T(8,128)} async-done(((f32[4,2,16,2048]{3,2,0,1:T(8,128)}), f32[4,2,16,256]{3,2,0,1:T(8,128)}) %reduce-scatter.2.cloned.1.call-update) | async-done | bytes 131088 | tf_op jit(solution)/shard_map/reduce_scatter | solution.py:173
  113.2 1.6 %copy.68 = f32[4,2,16,256]{3,2,1,0:T(8,128)} copy(f32[4,2,16,256]{3,2,0,1:T(8,128)} %reduce-scatter.2.cloned.1.call-done) | data formatting | bytes 262144 | tf_op jit(solution)/shard_map/reduce_scatter | solution.py:173
  114.7 3.7 %all-to-all-start.2 = ((f32[4,2,16,256]{3,2,1,0:T(8,128)}), f32[4,2,16,256]{3,2,1,0:T(8,128)S(1)}, u32[]{:S(2)}, u32[]{:S(2)}) async-start(f32[4,2,16,256]{3,2,1,0:T(8,128)} %copy.68), calls=%async_computation.3 | async-start | bytes 262144 | tf_op jit(solution)/shard_map/all_to_all | solution.py:174
  118.4 0.6 pad_maximum_fusion.3
  119.1 4.4 %all-to-all-done.2 = f32[4,2,16,256]{3,2,1,0:T(8,128)S(1)} async-done(((f32[4,2,16,256]{3,2,1,0:T(8,128)}), f32[4,2,16,256]{3,2,1,0:T(8,128)S(1)}, u32[]{:S(2)}, u32[]{:S(2)}) %all-to-all-start.2) | async-done | bytes 131104 | tf_op jit(solution)/shard_map/all_to_all | solution.py:174
  123.5 0.2 add_convert_fusion.2
  123.6 14.0 %all_gather.3 = bf16[32,2048]{1,0:T(8,128)(2,1)S(1)} all-gather(bf16[32,256]{1,0:T(8,128)(2,1)S(1)} %add_convert_fusion.2), channel_id=1, replica_groups=mesh['ep'=4,'tp'=8] {'tp'}, dimensions={1}, use_global_device_ids=true | all-gather | bytes 147456 | tf_op jit(solution)/shard_map/all_gather | solution.py:183
  137.6 0.7 copy.93
  (29 shorter events, 0.3 us)
Async XLA Ops:
  7.2 29.8 %copy-start = (bf16[256,2048]{1,0:T(8,128)(2,1)S(1)}, bf16[256,2048]{1,0:T(8,128)(2,1)}, u32[]{:S(2)}) copy-start(bf16[256,2048]{1,0:T(8,128)(2,1)} %param.30) | copy-start | bytes 3145732
  7.2 11.2 %copy-start.3 = (bf16[4,32,256]{2,1,0:T(8,128)(2,1)S(1)}, bf16[4,32,256]{2,1,0:T(8,128)(2,1)}, u32[]{:S(2)}) copy-start(bf16[4,32,256]{2,1,0:T(8,128)(2,1)} %param.23) | copy-start | bytes 196612
  7.2 11.8 %copy-start.2 = (bf16[4,32,2048]{2,1,0:T(8,128)(2,1)S(1)}, bf16[4,32,2048]{2,1,0:T(8,128)(2,1)}, u32[]{:S(2)}) copy-start(bf16[4,32,2048]{2,1,0:T(8,128)(2,1)} %param.21) | copy-start | bytes 1572868
  7.2 105.9 %reduce-scatter.2.cloned.1.call-start = ((), (), s32[]{:S(2)}) async-start(), calls=%async_computation.4 | async-start | bytes 1179648 | tf_op jit(solution)/shard_map/reduce_scatter | solution.py:173
  18.3 6.0 %copy-start.7 = (bf16[4,256]{1,0:T(4,128)(2,1)}, bf16[4,256]{1,0:T(4,128)(2,1)S(1)}, u32[]{:S(2)}) copy-start(bf16[4,256]{1,0:T(4,128)(2,1)S(1)} %get-tuple-element.27) | copy-start | bytes 6148
  21.3 16.0 %copy-start.5 = (s32[32,2]{0,1:T(2,128)S(1)}, s32[32,2]{0,1:T(2,128)}, u32[]{:S(2)}) copy-start(s32[32,2]{0,1:T(2,128)} %param.34) | copy-start | bytes 772
  21.3 26.8 %copy-start.6 = (bf16[2048]{0:T(1024)(128)(2,1)S(1)}, bf16[2048]{0:T(1024)(128)(2,1)}, u32[]{:S(2)}) copy-start(bf16[2048]{0:T(1024)(128)(2,1)} %param.31) | copy-start | bytes 12292
  21.3 40.0 %copy-start.1 = (bf16[32,2048]{1,0:T(8,128)(2,1)S(1)}, bf16[32,2048]{1,0:T(8,128)(2,1)}, u32[]{:S(2)}) copy-start(bf16[32,2048]{1,0:T(8,128)(2,1)} %param.19) | copy-start | bytes 393220
  24.4 37.2 %copy-start.8 = (bf16[2048,4]{0,1:T(4,128)(2,1)S(1)}, bf16[2048,4]{0,1:T(4,128)(2,1)}, u32[]{:S(2)}) copy-start(bf16[2048,4]{0,1:T(4,128)(2,1)} %param.32) | copy-start | bytes 49156
  24.4 37.4 %copy-start.4 = (bf16[2048,8]{0,1:T(8,128)(2,1)S(1)}, bf16[2048,8]{0,1:T(8,128)(2,1)}, u32[]{:S(2)}) copy-start(bf16[2048,8]{0,1:T(8,128)(2,1)} %param.33) | copy-start | bytes 98308
  37.2 1.6 %collective-permute-start = (f32[32,2048]{1,0:T(8,128)S(1)}, f32[32,2048]{1,0:T(8,128)S(1)}, u32[]{:S(2)}, u32[]{:S(2)}) collective-permute-start(f32[32,2048]{1,0:T(8,128)S(1)} %fusion.58), channel_id=1, source_target_pairs={{0,1},{1,0},{2,3},{3,2},{4,5},{5,4},{6,7},{7,6},{8,9},{9,8},{10,11... | collective-permute-start | bytes 786440 | tf_op jit(solution)/shard_map/ppermute | solution.py:21
  38.8 8.4 %collective-permute-start.1 = (f32[32,2048]{1,0:T(8,128)S(1)}, f32[32,2048]{1,0:T(8,128)S(1)}, u32[]{:S(2)}, u32[]{:S(2)}) collective-permute-start(f32[32,2048]{1,0:T(8,128)S(1)} %add.90), channel_id=1, source_target_pairs={{0,2},{1,3},{2,0},{3,1},{4,6},{5,7},{6,4},{7,5},{8,10},{9,11},{10,... | collective-permute-start | bytes 786440 | tf_op jit(solution)/shard_map/ppermute | solution.py:21
  47.3 14.1 %collective-permute-start.2 = (f32[32,2048]{1,0:T(8,128)S(1)}, f32[32,2048]{1,0:T(8,128)S(1)}, u32[]{:S(2)}, u32[]{:S(2)}) collective-permute-start(f32[32,2048]{1,0:T(8,128)S(1)} %add.91), channel_id=1, source_target_pairs={{0,4},{1,5},{2,6},{3,7},{4,0},{5,1},{6,2},{7,3},{8,12},{9,13},{10,... | collective-permute-start | bytes 786440 | tf_op jit(solution)/shard_map/ppermute | solution.py:21
  114.7 8.7 %all-to-all-start.2 = ((f32[4,2,16,256]{3,2,1,0:T(8,128)}), f32[4,2,16,256]{3,2,1,0:T(8,128)S(1)}, u32[]{:S(2)}, u32[]{:S(2)}) async-start(f32[4,2,16,256]{3,2,1,0:T(8,128)} %copy.68), calls=%async_computation.3 | async-start | bytes 262144 | tf_op jit(solution)/shard_map/all_to_all | solution.py:174
Sparse Core Ops, SparseCore 0:
  83.9 29.2 reduce-scatter.1
